TPU v7x, 128 devices: a whole 4x4x4 slice. The times are simulated.
128 devices in a mesh: sp: 16 (over z, x), tp: 8 (over y, core).
Axes of the slice: x: 4, y: 4, z: 4, core: 2. Of those that a mesh axis runs over, the one named last changes fastest.
Arguments:
- queries: bfloat16 [16384, 1024], P('sp', 'tp'), may hold values from -6 to 6, as said below
- key_rows: bfloat16 [16384, 1024], P('sp', 'tp'), may hold values from -6 to 6, as said below
- value_rows: bfloat16 [16384, 1024], P('sp', 'tp'), may hold values from -6 to 6
- lambdas: float32 [8], P('tp'), may hold values from 0.3 to 0.8
- head_gain: float32 [128], replicated, may hold values from 0.1 to 1.9
- out_weight: bfloat16 [1024, 2048], replicated, may hold values from -0.1875 to 0.1875
- stream: bfloat16 [16384, 2048], P(('sp', 'tp')), may hold values from -6 to 6
- ffn_gain: float32 [2048], replicated, may hold values from 0.1 to 1.9
- routes: int32 [16384, 2], P(('sp', 'tp')), may hold values from 0 to 15, all different within a row; in each aligned block of 128 rows (0 to 127, 128 to 255, ...) at most 20 rows name the same one
- route_weight: float32 [16384, 2], P(('sp', 'tp')), may hold values from 0.1 to 1
- gate_weight: bfloat16 [16, 2048, 5120], P('sp', None, 'tp'), may hold values from -0.125 to 0.125
- up_weight: bfloat16 [16, 2048, 5120], P('sp', None, 'tp'), may hold values from -0.125 to 0.125
- down_weight: bfloat16 [16, 5120, 2048], P('sp', 'tp'), may hold values from -0.078125 to 0.078125
Outputs:
- layer_out: bfloat16 [16384, 2048], P(('sp', 'tp'))
Inputs may be any that keep to these rules, and one draw needn't show every extreme that they name: Custom draw; the queries of a position meet only keys of the same or earlier positions. `key_rows`: custom draw. `routes`: each row names 2 different experts. In the 128 rows of one device no expert is named by more than 20 rows, and every draw reaches 20 on some device.
All inputs are finite; a program needn't handle non-finite values.
Results may differ from a plain program's by a relative error of at most 0.01.
Values may be sent and summed in bfloat16 or wider, within the bound.
No kernel may reach another device: no remote copies, remote signals or barrier semaphores. Data moves between devices by JAX's collectives and lax.ppermute only.
A program may use at most 128 MiB of HBM per device.

v0:
```python
import math
import jax
import jax.numpy as jnp
from jax import lax
from jax.sharding import PartitionSpec as P

DH = 64


def side_by_side(arrays, axis, dim, along):
    both = jnp.concatenate(arrays, axis=along)
    filled, at, gathered = (lax.all_gather(both, axis, axis=dim, tiled=True), 0, [])
    for a in arrays:
        gathered.append(lax.slice_in_dim(filled, at, at + a.shape[along], axis=along))
        at += a.shape[along]
    return tuple(gathered)


def expert_rows(rows_in, gate_local, up_local, down_local):
    flat = rows_in.reshape(-1, rows_in.shape[-1])
    gate = jnp.dot(flat, gate_local, preferred_element_type=jnp.float32)
    upper = jnp.dot(flat, up_local, preferred_element_type=jnp.float32)
    act = (jax.nn.silu(gate) * upper).astype(jnp.bfloat16)
    result = jnp.dot(act, down_local, preferred_element_type=jnp.float32)
    return result.reshape(rows_in.shape)


def local(
    queries,
    key_rows,
    value_rows,
    lambdas,
    head_gain,
    out_weight,
    stream,
    ffn_gain,
    routes,
    route_weight,
    gate_weight,
    up_weight,
    down_weight,
):
    length = queries.shape[0]
    head_count = queries.shape[1] // (2 * DH)
    query_heads = queries.reshape(length, head_count, 2, DH)
    offset = lax.axis_index("sp") * length
    query_pos = offset + jnp.arange(length, dtype=jnp.int32)
    last_pos = offset + length - 1
    scale = DH ** (-0.5)
    initial = (
        jnp.full((head_count, 2, length), -1e30, jnp.float32),
        jnp.zeros((head_count, 2, length), jnp.float32),
        jnp.zeros((head_count, 2, length, 2 * DH), jnp.float32),
    )
    key_piece, value_piece = side_by_side((key_rows, value_rows), "sp", 0, 1)
    count = key_piece.shape[0]
    block = math.gcd(count, 512)

    def advance(number, state):
        begin = number * block
        key_block = lax.dynamic_slice_in_dim(key_piece, begin, block, 0).reshape(
            block, head_count, 2, DH
        )
        value_block = lax.dynamic_slice_in_dim(value_piece, begin, block, 0).reshape(
            block, head_count, 2 * DH
        )
        key_pos = begin + jnp.arange(block, dtype=jnp.int32)

        def compute(inner):
            maxima, totals, accum = inner
            scores = (
                jnp.einsum(
                    "qhmd,khmd->hmqk", query_heads, key_block, preferred_element_type=jnp.float32
                )
                * scale
            )
            mask = key_pos[None, :] <= query_pos[:, None]
            scores = jnp.where(mask, scores, -jnp.inf)
            fresh = jnp.maximum(maxima, jnp.max(scores, axis=-1))
            expo = jnp.exp(scores - fresh[..., None])
            factor = jnp.exp(maxima - fresh)
            totals = totals * factor + jnp.sum(expo, axis=-1)
            accum = accum * factor[..., None] + jnp.einsum(
                "hmqk,khe->hmqe",
                expo.astype(jnp.bfloat16),
                value_block,
                preferred_element_type=jnp.float32,
            )
            return (fresh, totals, accum)

        return lax.cond(begin <= last_pos, compute, lambda inner: inner, state)

    maxima, totals, accum = lax.fori_loop(0, count // block, advance, initial)
    mixed = accum / totals[..., None]
    contrast = mixed[:, 0] - lambdas[:, None, None] * mixed[:, 1]
    contrast = (
        contrast
        * lax.rsqrt(jnp.mean(contrast * contrast, axis=-1, keepdims=True) + 1e-05)
        * head_gain
    )
    heads_out = (
        jnp.transpose(contrast, (1, 0, 2)).reshape(length, head_count * 2 * DH).astype(jnp.bfloat16)
    )
    heads_local = lax.all_to_all(heads_out, "tp", split_axis=0, concat_axis=1, tiled=True)
    attended = stream.astype(jnp.float32) + jnp.dot(
        heads_local, out_weight, preferred_element_type=jnp.float32
    )
    normed = (
        attended
        * lax.rsqrt(jnp.mean(attended * attended, axis=-1, keepdims=True) + 1e-06)
        * ffn_gain
    ).astype(jnp.bfloat16)
    rows_local = normed.shape[0]
    width = normed.shape[1]
    top_count = routes.shape[1]
    sp_size = lax.axis_size("sp")
    experts = sp_size * gate_weight.shape[0]
    slots = max(2, (rows_local * top_count * 5 + 4 * experts - 1) // (4 * experts))
    flat_routes = routes.reshape(-1)
    onehot = (flat_routes[:, None] == jnp.arange(experts, dtype=jnp.int32)[None, :]).astype(
        jnp.int32
    )
    before = jnp.cumsum(onehot, axis=0) - onehot
    slot = jnp.sum(before * onehot, axis=1)
    target = flat_routes * slots + slot
    placed = (target[:, None] == jnp.arange(experts * slots, dtype=jnp.int32)[None, :]).astype(
        jnp.float32
    )
    placed = placed.reshape(rows_local, top_count, experts * slots)
    dispatch = jnp.transpose(jnp.sum(placed, axis=1)).astype(jnp.bfloat16)
    combine = jnp.einsum("tk,tks->ts", route_weight, placed)
    outgoing = (
        jnp.dot(dispatch, normed, preferred_element_type=jnp.float32)
        .astype(jnp.bfloat16)
        .reshape(experts, slots, width)
    )
    gate_local = gate_weight[0]
    up_local = up_weight[0]
    down_local = down_weight[0]
    arrived = lax.all_to_all(outgoing, "sp", split_axis=0, concat_axis=0, tiled=True)
    partial_value = expert_rows(
        lax.all_gather(arrived[:, None], "tp", axis=1, tiled=True), gate_local, up_local, down_local
    )
    summed = lax.psum_scatter(
        partial_value.astype(jnp.bfloat16), "tp", scatter_dimension=1, tiled=True
    )
    returned = lax.all_to_all(summed, "sp", split_axis=0, concat_axis=0, tiled=True).reshape(
        experts * slots, width
    )
    routed = jnp.dot(combine, returned.astype(jnp.float32))
    return (attended + routed).astype(jnp.bfloat16)


def solution(mesh):
    placed = (
        P("sp", "tp"),
        P("sp", "tp"),
        P("sp", "tp"),
        P("tp"),
        P(),
        P(),
        P(("sp", "tp"), None),
        P(),
        P(("sp", "tp"), None),
        P(("sp", "tp"), None),
        P("sp", None, "tp"),
        P("sp", None, "tp"),
        P("sp", "tp", None),
    )
    return jax.shard_map(
        local, mesh=mesh, in_specs=placed, out_specs=P(("sp", "tp"), None), check_vma=False
    )
```

profile of v0, /device:TPU:9, one launch (start us, length us, event | category | flops | bytes accessed | tf_op | source)
XLA Modules:
  0.0 605.6 jit_solution(11017342687480843919)
XLA Ops:
  12.6 70.0 %all-gather.4.cloned.1.call-done = bf16[16384,256]{1,0:T(8,128)(2,1)} async-done(((bf16[1024,256]{1,0:T(8,128)(2,1)}), bf16[16384,256]{1,0:T(8,128)(2,1)}) %all-gather.4.cloned.1.call-update) | async-done | bytes 8388624 | tf_op jit(solution)/shard_map/all_gather | solution.py:12
  82.6 5.7 fusion.36
  88.3 6.4 %copy.89 = bf16[16384,128]{0,1:T(8,128)(2,1)} copy(bf16[16384,128]{1,0:T(8,128)(2,1)} %get-tuple-element.414) | data formatting | bytes 8388608
  95.7 16.0 %while.18 = (s32[]{:T(128)}, f32[1,2,1024]{2,1,0:T(2,128)S(1)}, f32[1,2,1024]{2,1,0:T(2,128)S(1)}, f32[1,2,1024,128]{3,2,1,0:T(8,128)}, s32[]{:T(128)}, /*index=...) while((s32[]{:T(128)}, f32[1,2,1024]{2,1,0:T(2,128)S(1)}, ...), condition=%wide.region_5.6_spmd.clone, body=%wide.region_0.5_spmd.clone.sunk | while | flops 415243776 | bytes 17719616 | solution.py:93
  95.7 7.0 %conditional.3 = ((f32[1,2,1024]{2,1,0:T(2,128)S(1)}, f32[1,2,1024]{2,1,0:T(2,128)S(1)}, f32[1,2,1024,128]{3,2,1,0:T(8,128)})) conditional(s32[]{:T(128)} %convert_element_type.84, (f32[1,2,1024]{2,1,0:T(2,128)S(1)}, f32[1,2,1024]{2,1,0:T(2,128)S(1)}, f32[1,2,1024,128]{3,2,1,0:T(8,128)}) %tuple.65, (s32[]{:T(128)}, s32[512]{0:T(512)S(1)}, s32[]{:T(128)}, ...), branch_computations={%region_1.0_spmd, %region_2.4_spmd} | conditional | flops 415243776 | bytes 17713234 | solution.py:91
  98.1 3.6 fusion.11
  102.8 7.0 %conditional.3 = ((f32[1,2,1024]{2,1,0:T(2,128)S(1)}, f32[1,2,1024]{2,1,0:T(2,128)S(1)}, f32[1,2,1024,128]{3,2,1,0:T(8,128)})) conditional(s32[]{:T(128)} %convert_element_type.84, (f32[1,2,1024]{2,1,0:T(2,128)S(1)}, f32[1,2,1024]{2,1,0:T(2,128)S(1)}, f32[1,2,1024,128]{3,2,1,0:T(8,128)}) %tuple.65, (s32[]{:T(128)}, s32[512]{0:T(512)S(1)}, s32[]{:T(128)}, ...), branch_computations={%region_1.0_spmd, %region_2.4_spmd} | conditional | flops 415243776 | bytes 17713234 | solution.py:91
  105.2 3.6 fusion.11
  114.6 5.3 all-to-all-start
  119.9 5.3 all-to-all-done
  125.4 3.1 multiply_reduce_fusion
  131.2 3.2 reshape.225
  134.4 235.9 %all_to_all.26 = bf16[16,20,2048]{2,1,0:T(8,128)(2,1)S(1)} all-to-all(bf16[16,20,2048]{2,1,0:T(8,128)(2,1)} %reshape.225), channel_id=1, replica_groups=mesh['sp'=16,'tp'=8] {'sp'}, dimensions={0} | all-to-all | bytes 2621440 | tf_op jit(solution)/shard_map/all_to_all | solution.py:140
  372.4 56.1 %all-gather.6.cloned.1.call-done = bf16[16,160,2048]{2,0,1:T(8,128)(2,1)} async-done(((bf16[16,20,2048]{2,0,1:T(8,128)(2,1)}), bf16[16,160,2048]{2,0,1:T(8,128)(2,1)}) %all-gather.6.cloned.1.call-update) | async-done | bytes 10485776 | tf_op jit(solution)/shard_map/all_gather | solution.py:142
  428.5 13.6 %copy.96 = bf16[16,160,2048]{2,1,0:T(8,128)(2,1)} copy(bf16[16,160,2048]{2,0,1:T(8,128)(2,1)} %all-gather.6.cloned.1.call-done) | data formatting | bytes 20971520 | tf_op jit(solution)/shard_map/all_gather | solution.py:142
  442.1 12.4 %fusion.24 = f32[2560,640]{1,0:T(8,128)S(1)} fusion(bf16[2560,2048]{1,0:T(8,128)(2,1)} %bitcast.85, bf16[1,2048,640]{2,1,0:T(8,128)(2,1)} %param.27), kind=kOutput, calls=%fused_computation.30 | convolution fusion | flops 6710886400 | bytes 19660800 | tf_op jit(solution)/shard_map/dot_general | solution.py:21
  454.5 10.4 %multiply_convert_fusion = bf16[2560,640]{1,0:T(8,128)(2,1)} fusion(f32[2560,640]{1,0:T(8,128)S(1)} %fusion.24, bf16[2560,2048]{1,0:T(8,128)(2,1)S(1)} %bitcast.86, bf16[1,2048,640]{2,1,0:T(8,128)(2,1)S(1)} %copy-done.7), kind=kOutput, calls=%fused_computation.26 | convolution fusion | flops 6720716800 | bytes 22937600 | tf_op jit(solution)/shard_map/dot_general | solution.py:22
  465.0 6.1 dot_general.36
  471.0 12.7 %convolution_convert_fusion = bf16[16,8,20,2048]{3,2,1,0:T(8,128)(2,1)S(1)} fusion(bf16[16,8,20,640]{3,2,1,0:T(8,128)(2,1)} %dot_general.36, bf16[1,640,2048]{2,1,0:T(8,128)(2,1)S(1)} %copy-done), kind=kOutput, calls=%fused_computation.25 | convolution fusion | flops 6716129280 | bytes 16384000 | tf_op jit(solution)/shard_map/dot_general | solution.py:24
  483.8 13.9 %copy.97 = bf16[16,8,20,2048]{3,0,2,1:T(8,128)(2,1)} copy(bf16[16,8,20,2048]{3,2,1,0:T(8,128)(2,1)S(1)} %convolution_convert_fusion) | data formatting | bytes 20971520 | tf_op jit(solution)/shard_map/convert_element_type | solution.py:145
  497.7 62.3 %reduce-scatter.2.cloned.1.call-done = bf16[16,1,20,2048]{3,0,2,1:T(8,128)(2,1)} async-done(((bf16[16,8,20,2048]{3,0,2,1:T(8,128)(2,1)}), bf16[16,1,20,2048]{3,0,2,1:T(8,128)(2,1)}) %reduce-scatter.2.cloned.1.call-update) | async-done | bytes 1310736 | tf_op jit(solution)/shard_map/reduce_scatter | solution.py:144
  562.0 30.9 %all_to_all.27 = bf16[16,1,20,2048]{3,2,1,0:T(8,128)(2,1)} all-to-all(bf16[16,1,20,2048]{3,2,1,0:T(8,128)(2,1)S(1)} %copy.98), channel_id=1, replica_groups=mesh['sp'=16,'tp'=8] {'sp'}, dimensions={0} | all-to-all | bytes 2621440 | tf_op jit(solution)/shard_map/all_to_all | solution.py:147
  592.9 3.3 reshape.227
  596.2 2.9 fusion.26
  (161 shorter events, 23.3 us)
Async XLA Ops:
  6.5 464.5 %copy-start = (bf16[1,640,2048]{2,1,0:T(8,128)(2,1)S(1)}, bf16[1,640,2048]{2,1,0:T(8,128)(2,1)}, u32[]{:S(2)}) copy-start(bf16[1,640,2048]{2,1,0:T(8,128)(2,1)} %param.29) | copy-start | bytes 7864324
  6.5 76.0 %all-gather.4.cloned.1.call-start = ((), (), s32[]{:S(2)}) async-start(), calls=%async_computation.4 | async-start | bytes 8912896 | tf_op jit(solution)/shard_map/all_gather | solution.py:12
  95.7 17.9 %copy-start.6 = (f32[128]{0:T(128)S(1)}, f32[128]{0:T(128)}, u32[]{:S(2)}) copy-start(f32[128]{0:T(128)} %param.21) | copy-start | bytes 1540
  111.8 8.0 %copy-start.4 = (s32[128,2]{0,1:T(2,128)S(1)}, s32[128,2]{0,1:T(2,128)}, u32[]{:S(2)}) copy-start(s32[128,2]{0,1:T(2,128)} %param.25) | copy-start | bytes 3076
  111.8 8.1 %copy-start.5 = (f32[128,2]{0,1:T(2,128)S(1)}, f32[128,2]{0,1:T(2,128)}, u32[]{:S(2)}) copy-start(f32[128,2]{0,1:T(2,128)} %param.26) | copy-start | bytes 3076
  113.6 15.9 %copy-start.3 = (f32[2048]{0:T(1024)S(1)}, f32[2048]{0:T(1024)}, u32[]{:S(2)}) copy-start(f32[2048]{0:T(1024)} %param.24) | copy-start | bytes 24580
  114.6 10.7 %all-to-all-start = ((bf16[8,128,128]{2,1,0:T(8,128)(2,1)}), bf16[8,128,128]{2,1,0:T(8,128)(2,1)S(1)}, u32[]{:S(2)}, u32[]{:S(2)}) async-start(bf16[8,128,128]{2,1,0:T(8,128)(2,1)} %multiply_convert_fusion.3), calls=%async_computation | async-start | bytes 524288 | tf_op jit(solution)/shard_map/all_to_all | solution.py:104
  119.8 308.6 %all-gather.6.cloned.1.call-start = ((), (), s32[]{:S(2)}) async-start(), calls=%async_computation.6 | async-start | bytes 11796480 | tf_op jit(solution)/shard_map/all_gather | solution.py:142
  128.5 1.0 copy-start.2
  372.1 187.9 %reduce-scatter.2.cloned.1.call-start = ((), (), s32[]{:S(2)}) async-start(), calls=%async_computation.5 | async-start | bytes 11796480 | tf_op jit(solution)/shard_map/reduce_scatter | solution.py:144
  442.1 12.5 %copy-start.1 = (bf16[16,160,2048]{2,1,0:T(8,128)(2,1)S(1)}, bf16[16,160,2048]{2,1,0:T(8,128)(2,1)}, u32[]{:S(2)}) copy-start(bf16[16,160,2048]{2,1,0:T(8,128)(2,1)} %copy.96) | copy-start | bytes 31457284
  442.1 12.5 %copy-start.7 = (bf16[1,2048,640]{2,1,0:T(8,128)(2,1)S(1)}, bf16[1,2048,640]{2,1,0:T(8,128)(2,1)}, u32[]{:S(2)}) copy-start(bf16[1,2048,640]{2,1,0:T(8,128)(2,1)} %param.28) | copy-start | bytes 7864324
Sparse Core Ops, SparseCore 0:
  9.5 73.0 all-gather.3
  372.2 56.1 all-gather.5
  497.8 62.1 reduce-scatter.1
where the time goes:
time: 608 us; the launch traced here: 606 us
  blocking collectives  267 us (44%)
  waiting for transfers between devices  194 us (32%)
  local copies, waits for them, and re-layouts  62.8 us (10%)
  matrix products  52.5 us (9%)
  between operations  14 us (2%)
  other arithmetic  8.29 us (1%)
    all_to_all x1, blocking collectives, local(): lax.all_to_all(outgoing, 'sp', split_axis=0, concat_axis=0, tiled=True)  236 us
    all_gather x1, waiting for transfers between devices, side_by_side(): lax.all_gather(both, axis, axis=dim, tiled=True)  70 us
    reduce_scatter x1, waiting for transfers between devices, local(): lax.psum_scatter(partial_value.astype(jnp.bfloat16), 'tp', scatter_dimens...  62.3 us
    all_gather x1, waiting for transfers between devices, local(): lax.all_gather(arrived[:, None], 'tp', axis=1, tiled=True)  56.1 us
    all_to_all x1, blocking collectives, local(): lax.all_to_all(summed, 'sp', split_axis=0, concat_axis=0, tiled=True)  30.9 us
    convert_element_type x1, local copies, waits for them, and re-layouts, local(): partial_value.astype(jnp.bfloat16)  13.9 us
    all_gather x1, local copies, waits for them, and re-layouts, local(): lax.all_gather(arrived[:, None], 'tp', axis=1, tiled=True)  13.6 us
    dot_general x1, matrix products, expert_rows(): result = jnp.dot(act, down_local, preferred_element_type=jnp.float32)  12.7 us
  transfers between devices with their start and end apart: 4, of which 4 were waited for; matrix products, arithmetic and copies ran while one was open for 1% of the time, Pallas kernels for 0%

commit v1 on v0

--- a/solution.py
+++ b/solution.py
@@ -139,7 +139,12 @@
     down_local = down_weight[0]
     arrived = lax.all_to_all(outgoing, "sp", split_axis=0, concat_axis=0, tiled=True)
     partial_value = expert_rows(
-        lax.all_gather(arrived[:, None], "tp", axis=1, tiled=True), gate_local, up_local, down_local
+        jnp.concatenate(
+            lax.all_to_all(jnp.stack([arrived[:, None]] * lax.axis_size("tp")), "tp", 0, 0), axis=1
+        ),
+        gate_local,
+        up_local,
+        down_local,
     )
     summed = lax.psum_scatter(
         partial_value.astype(jnp.bfloat16), "tp", scatter_dimension=1, tiled=True

time: 608 us -> 695 us (1.14)
  blocking collectives: 267 us -> 390 us
  waiting for transfers between devices: 194 us -> 133 us
  local copies, waits for them, and re-layouts: 62.8 us -> 86.5 us
    all_to_all x0 -> x1, blocking collectives: none -> 123 us  [local(): lax.all_to_all(jnp.stack([arrived[:, None]] * lax.axis_size('tp')), 'tp',...]
    all_gather x1 -> x0, waiting for transfers between devices: 56.1 us -> none  [local(): lax.all_gather(arrived[:, None], 'tp', axis=1, tiled=True)]
    another operation x1 -> x3, local copies, waits for them, and re-layouts: 0.01 us -> 21.8 us  [the longest x1 16.5 us: expert_rows(): flat = rows_in.reshape(-1, rows_in.shape[-1])]
    reshape x0 -> x1, local copies, waits for them, and re-layouts: none -> 16.8 us  [local(): jnp.concatenate(lax.all_to_all(jnp.stack([arrived[:, None]] * lax.axis_si...]
    all_gather x1 -> x0, local copies, waits for them, and re-layouts: 13.6 us -> none  [local(): lax.all_gather(arrived[:, None], 'tp', axis=1, tiled=True)]
  transfers between devices with their start and end apart: 4 -> 3, of which waited for: 4 -> 3; matrix products, arithmetic and copies ran while one was open for 1% -> 0% of each run, Pallas kernels for 0% -> 0%
where the time goes in v1:
time: 695 us; the launch traced here: 692 us
  blocking collectives  390 us (56%)
  waiting for transfers between devices  133 us (19%)
  local copies, waits for them, and re-layouts  86.5 us (12%)
  matrix products  52.5 us (8%)
  between operations  14.3 us (2%)
  other arithmetic  8.29 us (1%)
    all_to_all x1, blocking collectives, local(): lax.all_to_all(outgoing, 'sp', split_axis=0, concat_axis=0, tiled=True)  236 us
    all_to_all x1, blocking collectives, local(): lax.all_to_all(jnp.stack([arrived[:, None]] * lax.axis_size('tp')), 'tp',...  123 us
    all_gather x1, waiting for transfers between devices, side_by_side(): lax.all_gather(both, axis, axis=dim, tiled=True)  70 us
    reduce_scatter x1, waiting for transfers between devices, local(): lax.psum_scatter(partial_value.astype(jnp.bfloat16), 'tp', scatter_dimens...  58.1 us
    all_to_all x1, blocking collectives, local(): lax.all_to_all(summed, 'sp', split_axis=0, concat_axis=0, tiled=True)  30.9 us
    reshape x1, local copies, waits for them, and re-layouts, local(): jnp.concatenate(lax.all_to_all(jnp.stack([arrived[:, None]] * lax.axis_si...  16.8 us
    another operation x1, local copies, waits for them, and re-layouts, expert_rows(): flat = rows_in.reshape(-1, rows_in.shape[-1])  16.5 us
  transfers between devices with their start and end apart: 3, of which 3 were waited for; matrix products, arithmetic and copies ran while one was open for 0% of the time, Pallas kernels for 0%

profile of v1, /device:TPU:9, one launch (start us, length us, event | category | flops | bytes accessed | tf_op | source)
XLA Modules:
  0.0 692.5 jit_solution(8394809377020082909)
XLA Ops:
  12.6 70.0 %all-gather.2.cloned.1.call-done = bf16[16384,256]{1,0:T(8,128)(2,1)} async-done(((bf16[1024,256]{1,0:T(8,128)(2,1)}), bf16[16384,256]{1,0:T(8,128)(2,1)}) %all-gather.2.cloned.1.call-update) | async-done | bytes 8388624 | tf_op jit(solution)/shard_map/all_gather | solution.py:12
  82.6 5.7 fusion.36
  88.3 6.4 copy.77
  95.7 16.0 %while.18 = (s32[]{:T(128)}, f32[1,2,1024]{2,1,0:T(2,128)S(1)}, f32[1,2,1024]{2,1,0:T(2,128)S(1)}, f32[1,2,1024,128]{3,2,1,0:T(8,128)}, s32[]{:T(128)}, /*index=...) while((s32[]{:T(128)}, f32[1,2,1024]{2,1,0:T(2,128)S(1)}, ...), condition=%wide.region_5.6_spmd.clone, body=%wide.region_0.5_spmd.clone.sunk | while | flops 415243776 | bytes 17719616 | solution.py:93
  95.7 7.0 %conditional.3 = ((f32[1,2,1024]{2,1,0:T(2,128)S(1)}, f32[1,2,1024]{2,1,0:T(2,128)S(1)}, f32[1,2,1024,128]{3,2,1,0:T(8,128)})) conditional(s32[]{:T(128)} %convert_element_type.84, (f32[1,2,1024]{2,1,0:T(2,128)S(1)}, f32[1,2,1024]{2,1,0:T(2,128)S(1)}, f32[1,2,1024,128]{3,2,1,0:T(8,128)}) %tuple.64, (s32[]{:T(128)}, s32[512]{0:T(512)S(1)}, s32[]{:T(128)}, ...), branch_computations={%region_1.0_spmd, %region_2.4_spmd} | conditional | flops 415243776 | bytes 17713234 | solution.py:91
  98.1 3.6 fusion.11
  102.8 7.0 %conditional.3 = ((f32[1,2,1024]{2,1,0:T(2,128)S(1)}, f32[1,2,1024]{2,1,0:T(2,128)S(1)}, f32[1,2,1024,128]{3,2,1,0:T(8,128)})) conditional(s32[]{:T(128)} %convert_element_type.84, (f32[1,2,1024]{2,1,0:T(2,128)S(1)}, f32[1,2,1024]{2,1,0:T(2,128)S(1)}, f32[1,2,1024,128]{3,2,1,0:T(8,128)}) %tuple.64, (s32[]{:T(128)}, s32[512]{0:T(512)S(1)}, s32[]{:T(128)}, ...), branch_computations={%region_1.0_spmd, %region_2.4_spmd} | conditional | flops 415243776 | bytes 17713234 | solution.py:91
  105.2 3.6 fusion.11
  114.6 5.3 all-to-all-start
  119.9 5.3 all-to-all-done
  131.2 3.2 reshape.227
  134.4 235.9 %all_to_all.31 = bf16[16,20,2048]{2,1,0:T(8,128)(2,1)S(1)} all-to-all(bf16[16,20,2048]{2,1,0:T(8,128)(2,1)} %reshape.227), channel_id=1, replica_groups=mesh['sp'=16,'tp'=8] {'sp'}, dimensions={0} | all-to-all | bytes 2621440 | tf_op jit(solution)/shard_map/all_to_all | solution.py:140
  371.0 5.4 stack.3
  376.4 123.5 %all_to_all.32 = bf16[8,16,1,20,2048]{4,1,3,2,0:T(8,128)(2,1)S(1)} all-to-all(bf16[8,16,1,20,2048]{4,1,3,2,0:T(8,128)(2,1)} %stack.3), channel_id=1, replica_groups=mesh['sp'=16,'tp'=8] {'tp'}, dimensions={0} | all-to-all | bytes 20971520 | tf_op jit(solution)/shard_map/all_to_all | solution.py:143
  499.9 16.8 %copy.84 = bf16[16,8,1,20,2048]{4,3,1,0,2:T(8,128)(2,1)} copy(bf16[16,8,1,20,2048]{4,0,3,2,1:T(8,128)(2,1)S(1)} %bitcast.87) | data formatting | bytes 20971520 | tf_op jit(solution)/shard_map/reshape | solution.py:142
  516.7 16.5 %reshape_reshape.3 = bf16[2560,2048]{1,0:T(8,128)(2,1)} reshape(bf16[16,8,1,20,2048]{4,3,1,0,2:T(8,128)(2,1)} %copy.84) | data formatting | bytes 20971520 | tf_op jit(solution)/shard_map/reshape;reshape | solution.py:20
  533.2 12.4 %fusion.24 = f32[2560,640]{1,0:T(8,128)S(1)} fusion(bf16[2560,2048]{1,0:T(8,128)(2,1)} %reshape_reshape.3, bf16[1,2048,640]{2,1,0:T(8,128)(2,1)} %param.27), kind=kOutput, calls=%fused_computation.30 | convolution fusion | flops 6710886400 | bytes 19660800 | tf_op jit(solution)/shard_map/dot_general | solution.py:21
  545.6 10.4 %multiply_convert_fusion = bf16[2560,640]{1,0:T(8,128)(2,1)} fusion(f32[2560,640]{1,0:T(8,128)S(1)} %fusion.24, bf16[2560,2048]{1,0:T(8,128)(2,1)S(1)} %copy-done.1, bf16[1,2048,640]{2,1,0:T(8,128)(2,1)S(1)} %copy-done.7), kind=kOutput, calls=%fused_computation.26 | convolution fusion | flops 6720716800 | bytes 22937600 | tf_op jit(solution)/shard_map/dot_general | solution.py:22
  556.0 6.1 dot_general.36
  562.1 12.7 %convolution_convert_fusion = bf16[16,8,20,2048]{3,2,1,0:T(8,128)(2,1)S(1)} fusion(bf16[16,8,20,640]{3,2,1,0:T(8,128)(2,1)} %dot_general.36, bf16[1,640,2048]{2,1,0:T(8,128)(2,1)S(1)} %copy-done), kind=kOutput, calls=%fused_computation.25 | convolution fusion | flops 6716129280 | bytes 16384000 | tf_op jit(solution)/shard_map/dot_general | solution.py:24
  574.8 13.6 %copy.85 = bf16[16,8,20,2048]{3,0,2,1:T(8,128)(2,1)} copy(bf16[16,8,20,2048]{3,2,1,0:T(8,128)(2,1)S(1)} %convolution_convert_fusion) | data formatting | bytes 20971520 | tf_op jit(solution)/shard_map/convert_element_type | solution.py:150
  588.5 58.1 %reduce-scatter.2.cloned.1.call-done = bf16[16,1,20,2048]{3,0,2,1:T(8,128)(2,1)} async-done(((bf16[16,8,20,2048]{3,0,2,1:T(8,128)(2,1)}), bf16[16,1,20,2048]{3,0,2,1:T(8,128)(2,1)}) %reduce-scatter.2.cloned.1.call-update) | async-done | bytes 1310736 | tf_op jit(solution)/shard_map/reduce_scatter | solution.py:149
  648.6 30.9 %all_to_all.33 = bf16[16,1,20,2048]{3,2,1,0:T(8,128)(2,1)} all-to-all(bf16[16,1,20,2048]{3,2,1,0:T(8,128)(2,1)S(1)} %copy.86), channel_id=1, replica_groups=mesh['sp'=16,'tp'=8] {'sp'}, dimensions={0} | all-to-all | bytes 2621440 | tf_op jit(solution)/shard_map/all_to_all | solution.py:152
  679.5 3.3 reshape.229
  (161 shorter events, 28.0 us)
Async XLA Ops:
  6.5 555.6 %copy-start = (bf16[1,640,2048]{2,1,0:T(8,128)(2,1)S(1)}, bf16[1,640,2048]{2,1,0:T(8,128)(2,1)}, u32[]{:S(2)}) copy-start(bf16[1,640,2048]{2,1,0:T(8,128)(2,1)} %param.29) | copy-start | bytes 7864324
  6.5 76.0 %all-gather.2.cloned.1.call-start = ((), (), s32[]{:S(2)}) async-start(), calls=%async_computation.5 | async-start | bytes 8912896 | tf_op jit(solution)/shard_map/all_gather | solution.py:12
  95.7 17.9 %copy-start.6 = (f32[128]{0:T(128)S(1)}, f32[128]{0:T(128)}, u32[]{:S(2)}) copy-start(f32[128]{0:T(128)} %param.21) | copy-start | bytes 1540
  111.8 8.0 %copy-start.4 = (s32[128,2]{0,1:T(2,128)S(1)}, s32[128,2]{0,1:T(2,128)}, u32[]{:S(2)}) copy-start(s32[128,2]{0,1:T(2,128)} %param.25) | copy-start | bytes 3076
  111.8 8.1 %copy-start.5 = (f32[128,2]{0,1:T(2,128)S(1)}, f32[128,2]{0,1:T(2,128)}, u32[]{:S(2)}) copy-start(f32[128,2]{0,1:T(2,128)} %param.26) | copy-start | bytes 3076
  113.6 15.9 %copy-start.3 = (f32[2048]{0:T(1024)S(1)}, f32[2048]{0:T(1024)}, u32[]{:S(2)}) copy-start(f32[2048]{0:T(1024)} %param.24) | copy-start | bytes 24580
  114.6 10.7 %all-to-all-start = ((bf16[8,128,128]{2,1,0:T(8,128)(2,1)}), bf16[8,128,128]{2,1,0:T(8,128)(2,1)S(1)}, u32[]{:S(2)}, u32[]{:S(2)}) async-start(bf16[8,128,128]{2,1,0:T(8,128)(2,1)} %multiply_convert_fusion.3), calls=%async_computation | async-start | bytes 524288 | tf_op jit(solution)/shard_map/all_to_all | solution.py:104
  119.8 526.7 %reduce-scatter.2.cloned.1.call-start = ((), (), s32[]{:S(2)}) async-start(), calls=%async_computation.6 | async-start | bytes 11796480 | tf_op jit(solution)/shard_map/reduce_scatter | solution.py:149
  128.5 1.0 copy-start.2
  533.2 12.4 %copy-start.1 = (bf16[2560,2048]{1,0:T(8,128)(2,1)S(1)}, bf16[2560,2048]{1,0:T(8,128)(2,1)}, u32[]{:S(2)}) copy-start(bf16[2560,2048]{1,0:T(8,128)(2,1)} %reshape_reshape.3) | copy-start | bytes 31457284
  533.2 12.4 %copy-start.7 = (bf16[1,2048,640]{2,1,0:T(8,128)(2,1)S(1)}, bf16[1,2048,640]{2,1,0:T(8,128)(2,1)}, u32[]{:S(2)}) copy-start(bf16[1,2048,640]{2,1,0:T(8,128)(2,1)} %param.28) | copy-start | bytes 7864324
Sparse Core Ops, SparseCore 0:
  9.5 73.0 all-gather.1
  588.6 57.8 reduce-scatter.1
